TPU v7x, 32 devices: a whole 2x2x4 slice. The times are simulated.
32 devices in a mesh: ep: 4 (over y, x), tp: 8 (over z, core).
Axes of the slice: x: 2, y: 2, z: 4, core: 2. Of those that a mesh axis runs over, the one named last changes fastest.
Arguments:
- tokens: bfloat16 [64, 4096], P('ep'), may hold values from -6 to 6
- attn_gain: float32 [4096], replicated, may hold values from 0.1 to 1.9
- w_query: bfloat16 [4096, 2048], P('ep', 'tp'), may hold values from -0.15625 to 0.15625
- w_key: bfloat16 [4096, 2048], P('ep', 'tp'), may hold values from -0.09375 to 0.09375
- w_value: bfloat16 [4096, 2048], P('ep', 'tp'), may hold values from -0.09375 to 0.09375
- mix_lambda: float32 [16], P('tp'), may hold values from 0.3 to 0.8
- head_gain: float32 [128], replicated, may hold values from 0.1 to 1.9
- w_output: bfloat16 [2048, 4096], P('tp'), may hold values from -0.125 to 0.125
- cache_keys: bfloat16 [64, 1024, 2048], P('ep', None, 'tp'), may hold values from -180 to 180
- cache_value: bfloat16 [64, 1024, 2048], P('ep', None, 'tp'), may hold values from -6 to 6
- lengths: int32 [64], P('ep'), may hold values from 1 to 1024
- moe_gain: float32 [4096], replicated, may hold values from 0.1 to 1.9
- group_ids: int32 [64], P('ep'), may hold values from 0 to 1, as said below
- member_ids: int32 [64, 2], P('ep'), may hold values from 0 to 1, as said below
- group_gate: float32 [64], P('ep'), may hold values from 0.3 to 1
- member_logits: float32 [64, 2], P('ep'), may hold values from -4 to 4
- w_exp_gate: bfloat16 [4, 4096, 2048], P('ep', None, 'tp'), may hold values from -0.09375 to 0.09375
- w_exp_up: bfloat16 [4, 4096, 2048], P('ep', None, 'tp'), may hold values from -0.09375 to 0.09375
- w_exp_down: bfloat16 [4, 2048, 4096], P('ep', 'tp'), may hold values from -0.125 to 0.125
Outputs:
- mixed: bfloat16 [64, 4096], P('ep', 'tp')
- fresh_keys: bfloat16 [64, 2048], P('ep', 'tp')
- fresh_value: bfloat16 [64, 2048], P('ep', 'tp')
Inputs may be any that keep to these rules, and one draw needn't show every extreme that they name: `group_ids`: each index of ep holds 16 consecutive tokens, of which every group gets the same number. A token's 2 members differ, and every expert group_ids * 2 + member_ids receives exactly 8 of the token-expert pairs of each index of ep.
All inputs are finite; a program needn't handle non-finite values.
Results may differ from a plain program's by a relative error of at most 0.015.
The roundings to bfloat16 on the way count: a program that leaves them out, or rounds other values in their place, can miss the bound.
Values may be sent and summed in bfloat16 or wider, within the bound.
A program may use at most 64 MiB of HBM per device.

v0:
```python
import jax
import jax.numpy as jnp
from jax import lax
from jax.sharding import PartitionSpec as P

EPG = 2
EPS = 1e-06


def rms_scale(values, gain):
    return values * lax.rsqrt(jnp.mean(values * values, axis=-1, keepdims=True) + EPS) * gain


def on_device(
    tokens,
    attn_gain,
    w_query,
    w_key,
    w_value,
    mix_lambda,
    head_gain,
    w_output,
    cache_keys,
    cache_value,
    lengths,
    moe_gain,
    group_ids,
    member_ids,
    group_gate,
    member_logits,
    w_exp_gate,
    w_exp_up,
    w_exp_down,
):
    seqs, width = tokens.shape
    resid_in = tokens.astype(jnp.float32)
    normed = rms_scale(resid_in, attn_gain).astype(jnp.bfloat16)
    heads_local = mix_lambda.shape[0]
    qk_cols = w_query.shape[1]
    head_dim = qk_cols // (2 * heads_local)
    stacked = jnp.concatenate([w_query, w_key, w_value], axis=1)
    sliced = lax.all_to_all(normed, "ep", split_axis=1, concat_axis=0, tiled=True)
    projected = lax.psum_scatter(
        jnp.dot(sliced, stacked, preferred_element_type=jnp.float32),
        "ep",
        scatter_dimension=0,
        tiled=True,
    )
    projected = projected.astype(jnp.bfloat16)
    query = projected[:, :qk_cols]
    fresh_keys = projected[:, qk_cols : 2 * qk_cols]
    fresh_value = projected[:, 2 * qk_cols :]
    positions_all = cache_keys.shape[1]
    total_heads = heads_local * lax.axis_size("tp")
    head_index = (lax.axis_index("tp") * heads_local + jnp.arange(heads_local)).astype(jnp.float32)
    slopes = 2.0 ** (-8.0 * (head_index + 1.0) / total_heads)
    scale = head_dim ** (-0.5)
    positions = jnp.arange(positions_all)
    dist = (lengths[:, None] - positions[None, :]).astype(jnp.float32)
    valid = positions[None, :] < lengths[:, None]
    query4 = query.reshape(seqs, heads_local, 2, head_dim)
    keys5 = cache_keys.reshape(seqs, positions_all, heads_local, 2, head_dim)
    old = jnp.einsum("shcd,slhcd->cshl", query4, keys5, preferred_element_type=jnp.float32) * scale
    old = old - slopes[None, None, :, None] * dist[None, :, None, :]
    old = jnp.where(valid[None, :, None, :], old, -jnp.inf)
    fresh4 = fresh_keys.reshape(seqs, heads_local, 2, head_dim).astype(jnp.float32)
    new = jnp.moveaxis(jnp.sum(query4.astype(jnp.float32) * fresh4, axis=-1) * scale, 2, 0)
    full = jnp.concatenate([old, new[..., None]], axis=-1)
    maps = jax.nn.softmax(full, axis=-1)
    weights = (maps[0] - mix_lambda[None, :, None] * maps[1]).astype(jnp.bfloat16)
    values = cache_value.reshape(seqs, positions_all, heads_local, 2 * head_dim)
    head_mix = jnp.einsum(
        "shl,slhe->she", weights[..., :positions_all], values, preferred_element_type=jnp.float32
    )
    head_mix = head_mix + weights[..., positions_all].astype(jnp.float32)[
        ..., None
    ] * fresh_value.reshape(seqs, heads_local, 2 * head_dim).astype(jnp.float32)
    head_out = (
        rms_scale(head_mix, head_gain)
        .astype(jnp.bfloat16)
        .reshape(seqs, heads_local * 2 * head_dim)
    )
    term = jnp.dot(head_out, w_output, preferred_element_type=jnp.float32).astype(jnp.bfloat16)
    attn_sum = lax.psum(
        lax.optimization_barrier(term).astype(jnp.float32).astype(jnp.bfloat16), "tp"
    ).astype(jnp.float32)
    resid = resid_in + attn_sum
    moe_in = rms_scale(resid, moe_gain).astype(jnp.bfloat16)
    top = member_ids.shape[1]
    experts_local = w_exp_gate.shape[0]
    ep_count = lax.axis_size("ep")
    experts_all = experts_local * ep_count
    capacity = seqs * top // experts_all
    expert_ids = group_ids[:, None] * EPG + member_ids
    route_weight = jax.nn.softmax(member_logits, axis=-1) * group_gate[:, None]
    flat_ids = expert_ids.reshape(seqs * top)
    onehot = (flat_ids[:, None] == jnp.arange(experts_all)[None, :]).astype(jnp.int32)
    ranks = jnp.sum(jnp.cumsum(onehot, axis=0) * onehot, axis=1) - 1
    slot_grid = (flat_ids * capacity + ranks).reshape(seqs, top)
    slot_range = jnp.arange(experts_all * capacity)
    picker = jnp.sum((slot_grid[None, :, :] == slot_range[:, None, None]).astype(jnp.int32), axis=2)
    dispatch = jnp.dot(
        picker.astype(jnp.bfloat16), moe_in, preferred_element_type=jnp.float32
    ).astype(jnp.bfloat16)
    dispatch = dispatch.reshape(ep_count, experts_local, capacity, width)
    received = lax.all_to_all(dispatch, "ep", split_axis=0, concat_axis=2, tiled=True)
    received = received.reshape(experts_local, ep_count * capacity, width)
    gate = jnp.einsum("erd,edf->erf", received, w_exp_gate, preferred_element_type=jnp.float32)
    upper = jnp.einsum("erd,edf->erf", received, w_exp_up, preferred_element_type=jnp.float32)
    hidden = (jax.nn.silu(gate) * upper).astype(jnp.bfloat16)
    down = jnp.einsum("erf,efd->erd", hidden, w_exp_down, preferred_element_type=jnp.float32)
    summed = lax.psum_scatter(down.astype(jnp.bfloat16), "tp", scatter_dimension=2, tiled=True)
    cols = summed.shape[2]
    returned = lax.all_to_all(
        summed.reshape(experts_local, ep_count, capacity, cols),
        "ep",
        split_axis=1,
        concat_axis=0,
        tiled=True,
    )
    returned = returned.reshape(experts_all * capacity, cols)
    picked = returned[slot_grid].astype(jnp.float32)
    routed = jnp.sum(picked * route_weight[:, :, None], axis=1)
    own = lax.dynamic_slice_in_dim(resid, lax.axis_index("tp") * cols, cols, 1)
    mixed = (own + routed).astype(jnp.bfloat16)
    return (mixed, fresh_keys, fresh_value)


def solution(mesh):
    return jax.shard_map(
        on_device,
        mesh=mesh,
        in_specs=(
            P("ep", None),
            P(),
            P("ep", "tp"),
            P("ep", "tp"),
            P("ep", "tp"),
            P("tp"),
            P(),
            P("tp", None),
            P("ep", None, "tp"),
            P("ep", None, "tp"),
            P("ep"),
            P(),
            P("ep"),
            P("ep", None),
            P("ep"),
            P("ep", None),
            P("ep", None, "tp"),
            P("ep", None, "tp"),
            P("ep", "tp", None),
        ),
        out_specs=(P("ep", "tp"), P("ep", "tp"), P("ep", "tp")),
        check_vma=False,
    )
```

profile of v0, /device:TPU:0, one launch (start us, length us, event | category | flops | bytes accessed | tf_op | source)
XLA Modules:
  0.0 177.5 jit_solution(10258000634573673739)
XLA Ops:
  7.2 1.2 fusion.27
  8.4 1.0 fusion.29
  9.4 0.6 copy.110
  10.0 5.2 %all-to-all-start = ((bf16[16,4,1024]{2,0,1:T(8,128)(2,1)}), bf16[16,4,1024]{2,0,1:T(8,128)(2,1)S(1)}, u32[]{:S(2)}, u32[]{:S(2)}) async-start(bf16[16,4,1024]{2,0,1:T(8,128)(2,1)} %bitcast.80), calls=%async_computation | async-start | bytes 262144 | tf_op jit(solution)/shard_map/all_to_all | solution.py:42
  15.2 0.7 subtract_convert_fusion
  16.0 0.8 copy.78
  16.7 0.7 broadcast_multiply_fusion.1
  17.5 0.1 eq.28
  17.7 0.2 select_reduce_fusion
  17.9 0.1 sub.53
  18.0 0.1 compare_select_fusion
  18.0 2.2 %all-to-all-done = bf16[16,4,1024]{2,0,1:T(8,128)(2,1)S(1)} async-done(((bf16[16,4,1024]{2,0,1:T(8,128)(2,1)}), bf16[16,4,1024]{2,0,1:T(8,128)(2,1)S(1)}, u32[]{:S(2)}, u32[]{:S(2)}) %all-to-all-start) | async-done | bytes 131104 | tf_op jit(solution)/shard_map/all_to_all | solution.py:42
  20.3 2.5 %fusion.12 = f32[64,768]{1,0:T(8,128)} fusion(bf16[64,1024]{1,0:T(8,128)(2,1)S(1)} %bitcast.84, bf16[1024,256]{1,0:T(8,128)(2,1)} %param.23, bf16[1024,256]{1,0:T(8,128)(2,1)} %param.22, bf16[1024,256]{1,0:T(8,128)(2,1)} %param.21), kind=kOutput, calls=%fused_computation.16 | convolution fusion | flops 105381888 | bytes 1900544 | tf_op jit(solution)/shard_map/dot_general | solution.py:44
  22.8 0.1 iota_compare_fusion
  22.9 12.3 %copy.74 = bf16[16,1024,256]{1,2,0:T(8,128)(2,1)} copy(bf16[16,1024,256]{2,1,0:T(8,128)(2,1)} %param.27) | data formatting | bytes 16777216 | tf_op args[8]
  35.2 0.1 copy.79
  35.3 0.1 broadcast_multiply_fusion
  35.4 11.5 %reduce-scatter.3.cloned.1.call-done = f32[16,768]{1,0:T(8,128)} async-done(((f32[64,768]{1,0:T(8,128)}), f32[16,768]{1,0:T(8,128)}) %reduce-scatter.3.cloned.1.call-update) | async-done | bytes 49168 | tf_op jit(solution)/shard_map/reduce_scatter | solution.py:43
  46.9 0.8 convert_element_type.87
  47.7 0.1 reshape.176
  47.8 0.1 reshape.201
  47.9 0.1 reshape.187
  48.0 0.1 multiply_reduce_fusion.2
  48.1 0.1 copy.75
  48.2 4.6 %fusion.3 = f32[2,16,2,1,1024]{4,3,2,1,0:T(1,128)S(1)} fusion(bf16[16,1024,2,2,64]{1,4,3,2,0:T(8,128)(2,1)} %bitcast.81, bf16[16,2,2,64,1]{3,2,1,0,4:T(2,128)(2,1)S(1)} %reshape.201), kind=kOutput, calls=%fused_computation.4 | convolution fusion | flops 8388608 | bytes 8658944 | tf_op jit(solution)/shard_map/shcd,slhcd->cshl/dot_general | solution.py:63
  52.8 0.2 fusion.66
  53.0 0.1 copy.76
  53.1 0.8 fusion.35
  53.9 0.1 fusion.39
  54.1 0.2 copy.89
  54.3 4.7 %fusion = f32[16,2,1,128]{3,2,1,0:T(1,128)S(1)} fusion(bf16[16,2,1024,1]{2,0,1,3:T(8,128)(2,1)S(1)} %slice_bitcast_fusion.2, bf16[16,1024,256]{2,1,0:T(8,128)(2,1)} %param.28), kind=kOutput, calls=%fused_computation.1 | convolution fusion | flops 8388608 | bytes 8470528 | tf_op jit(solution)/shard_map/shl,slhe->she/dot_general | solution.py:72
  59.0 0.2 multiply_reduce_fusion.3
  59.2 0.1 multiply_convert_fusion.2
  59.3 1.0 convolution_convert_fusion.2
  60.5 55.0 %all-reduce.2.cloned.1.call-done = bf16[16,4096]{1,0:T(8,128)(2,1)} async-done(((bf16[16,4096]{1,0:T(8,128)(2,1)}), bf16[16,4096]{1,0:T(8,128)(2,1)}) %all-reduce.2.cloned.1.call-update) | async-done | bytes 131088 | tf_op jit(solution)/shard_map/psum | solution.py:84
  115.5 1.1 convert_add_fusion
  116.6 1.2 fusion.5
  117.8 9.2 %all_to_all.37 = bf16[4,1,8,4096]{3,2,1,0:T(8,128)(2,1)S(1)} all-to-all(bf16[4,1,8,4096]{3,2,1,0:T(8,128)(2,1)S(1)} %fusion.5), channel_id=1, replica_groups=mesh['ep'=4,'tp'=8] {'ep'}, dimensions={0} | all-to-all | bytes 524288 | tf_op jit(solution)/shard_map/all_to_all | solution.py:106
  126.9 2.0 %fusion.10 = f32[32,256]{1,0:T(8,128)S(1)} fusion(bf16[1,4096,256]{2,1,0:T(8,128)(2,1)} %param.35, bf16[4,1,8,4096]{3,2,1,0:T(8,128)(2,1)S(1)} %all_to_all.37), kind=kOutput, calls=%fused_computation.14 | convolution fusion | flops 67108864 | bytes 2392064 | tf_op jit(solution)/shard_map/erd,edf->erf/dot_general | solution.py:108
  129.0 3.6 %fusion.6 = bf16[1,32,4096]{2,1,0:T(8,128)(2,1)} fusion(bf16[1,256,4096]{2,1,0:T(8,128)(2,1)S(1)} %copy-done, bf16[1,4096,256]{2,1,0:T(8,128)(2,1)} %param.36, bf16[4,1,8,4096]{3,2,1,0:T(8,128)(2,1)S(1)} %all_to_all.37, f32[32,256]{1,0:T(8,128)S(1)} %fusion.10), kind=kOutput, calls=%fused_computation.9 | convolution fusion | flops 134397952 | bytes 4751360 | tf_op jit(solution)/shard_map/erf,efd->erd/dot_general | solution.py:111
  132.6 0.1 reshape.192
  132.8 28.4 %reduce-scatter.5.cloned.1.call-done = bf16[1,32,512]{2,1,0:T(8,128)(2,1)} async-done(((bf16[1,32,4096]{2,1,0:T(8,128)(2,1)}), bf16[1,32,512]{2,1,0:T(8,128)(2,1)}) %reduce-scatter.5.cloned.1.call-update) | async-done | bytes 32784 | tf_op jit(solution)/shard_map/reduce_scatter | solution.py:112
  161.1 3.7 %all-to-all-start.2 = ((bf16[1,4,8,512]{3,2,0,1:T(8,128)(2,1)}), bf16[1,4,8,512]{3,2,0,1:T(8,128)(2,1)S(1)}, u32[]{:S(2)}, u32[]{:S(2)}) async-start(bf16[1,4,8,512]{3,2,0,1:T(8,128)(2,1)} %bitcast.90), calls=%async_computation.4 | async-start | bytes 65536 | tf_op jit(solution)/shard_map/all_to_all | solution.py:114
  164.8 0.1 copy.82
  164.9 4.7 %all-to-all-done.2 = bf16[1,4,8,512]{3,2,0,1:T(8,128)(2,1)S(1)} async-done(((bf16[1,4,8,512]{3,2,0,1:T(8,128)(2,1)}), bf16[1,4,8,512]{3,2,0,1:T(8,128)(2,1)S(1)}, u32[]{:S(2)}, u32[]{:S(2)}) %all-to-all-start.2) | async-done | bytes 32800 | tf_op jit(solution)/shard_map/all_to_all | solution.py:114
  169.5 0.6 gather_fusion
  170.2 0.1 multiply_reduce_fusion.1
  170.4 0.6 add_convert_fusion
  (48 shorter events, 0.7 us)
Async XLA Ops:
  7.2 121.8 %copy-start = (bf16[1,256,4096]{2,1,0:T(8,128)(2,1)S(1)}, bf16[1,256,4096]{2,1,0:T(8,128)(2,1)}, u32[]{:S(2)}) copy-start(bf16[1,256,4096]{2,1,0:T(8,128)(2,1)} %param.37) | copy-start | bytes 6291460
  10.0 10.2 %all-to-all-start = ((bf16[16,4,1024]{2,0,1:T(8,128)(2,1)}), bf16[16,4,1024]{2,0,1:T(8,128)(2,1)S(1)}, u32[]{:S(2)}, u32[]{:S(2)}) async-start(bf16[16,4,1024]{2,0,1:T(8,128)(2,1)} %bitcast.80), calls=%async_computation | async-start | bytes 262144 | tf_op jit(solution)/shard_map/all_to_all | solution.py:42
  15.2 31.7 %reduce-scatter.3.cloned.1.call-start = ((), (), s32[]{:S(2)}) async-start(), calls=%async_computation.5 | async-start | bytes 245760 | tf_op jit(solution)/shard_map/reduce_scatter | solution.py:43
  20.3 2.6 %copy-start.7 = (s32[16]{0:T(128)S(1)}, s32[16]{0:T(128)}, u32[]{:S(2)}) copy-start(s32[16]{0:T(128)} %param.29) | copy-start | bytes 196
  22.8 92.7 %all-reduce.2.cloned.1.call-start = ((), (), s32[]{:S(2)}) async-start(), calls=%async_computation.6 | async-start | bytes 262144 | tf_op jit(solution)/shard_map/psum | solution.py:84
  47.7 5.1 %copy-start.4 = (bf16[16,256]{1,0:T(8,128)(2,1)}, bf16[16,256]{1,0:T(8,128)(2,1)S(1)}, u32[]{:S(2)}) copy-start(bf16[16,256]{1,0:T(8,128)(2,1)S(1)} %get-tuple-element.10) | copy-start | bytes 24580
  47.7 6.5 %copy-start.3 = (bf16[16,256]{1,0:T(8,128)(2,1)}, bf16[16,256]{1,0:T(8,128)(2,1)S(1)}, u32[]{:S(2)}) copy-start(bf16[16,256]{1,0:T(8,128)(2,1)S(1)} %get-tuple-element.9) | copy-start | bytes 24580
  52.8 1.1 copy-start.8
  54.3 4.9 %copy-start.9 = (f32[128]{0:T(128)S(1)}, f32[128]{0:T(128)}, u32[]{:S(2)}) copy-start(f32[128]{0:T(128)} %param.25) | copy-start | bytes 1540
  54.3 5.0 %copy-start.2 = (bf16[256,4096]{1,0:T(8,128)(2,1)S(1)}, bf16[256,4096]{1,0:T(8,128)(2,1)}, u32[]{:S(2)}) copy-start(bf16[256,4096]{1,0:T(8,128)(2,1)} %param.26) | copy-start | bytes 6291460
  59.0 56.5 %copy-start.1 = (bf16[16,4096]{1,0:T(8,128)(2,1)S(1)}, bf16[16,4096]{1,0:T(8,128)(2,1)}, u32[]{:S(2)}) copy-start(bf16[16,4096]{1,0:T(8,128)(2,1)} %param.19) | copy-start | bytes 393220
  59.0 57.5 %copy-start.5 = (f32[4096]{0:T(1024)S(1)}, f32[4096]{0:T(1024)}, u32[]{:S(2)}) copy-start(f32[4096]{0:T(1024)} %param.30) | copy-start | bytes 49156
  60.4 100.7 %reduce-scatter.5.cloned.1.call-start = ((), (), s32[]{:S(2)}) async-start(), calls=%async_computation.7 | async-start | bytes 294912 | tf_op jit(solution)/shard_map/reduce_scatter | solution.py:112
  129.0 3.7 %copy-start.6 = (f32[16,2]{0,1:T(2,128)S(1)}, f32[16,2]{0,1:T(2,128)}, u32[]{:S(2)}) copy-start(f32[16,2]{0,1:T(2,128)} %param.34) | copy-start | bytes 388
  129.0 3.8 %copy-start.10 = (f32[16]{0:T(128)S(1)}, f32[16]{0:T(128)}, u32[]{:S(2)}) copy-start(f32[16]{0:T(128)} %param.33) | copy-start | bytes 196
  161.1 8.4 %all-to-all-start.2 = ((bf16[1,4,8,512]{3,2,0,1:T(8,128)(2,1)}), bf16[1,4,8,512]{3,2,0,1:T(8,128)(2,1)S(1)}, u32[]{:S(2)}, u32[]{:S(2)}) async-start(bf16[1,4,8,512]{3,2,0,1:T(8,128)(2,1)} %bitcast.90), calls=%async_computation.4 | async-start | bytes 65536 | tf_op jit(solution)/shard_map/all_to_all | solution.py:114
Sparse Core Ops, SparseCore 0:
  22.9 23.9 reduce-scatter.2
  60.5 54.9 all-reduce.1
  132.7 28.3 reduce-scatter.4
where the time goes:
time: 178 us
  waiting for transfers between devices  102 us (57%)
  matrix products  19.6 us (11%)
  local copies, waits for them, and re-layouts  15.5 us (9%)
  between operations  14 us (8%)
  blocking collectives  9.17 us (5%)
  starting transfers between devices  8.93 us (5%)
  other arithmetic  8.5 us (5%)
    psum x1, waiting for transfers between devices, on_device(): lax.psum(lax.optimization_barrier(term).astype(jnp.float32).astype(jnp.bf...  55 us
    reduce_scatter x1, waiting for transfers between devices, on_device(): lax.psum_scatter(down.astype(jnp.bfloat16), 'tp', scatter_dimension=2, ti...  28.4 us
    unnamed x24, local copies, waits for them, and re-layouts  13.1 us
    reduce_scatter x1, waiting for transfers between devices, on_device(): lax.psum_scatter(jnp.dot(sliced, stacked, preferred_element_type=jnp.floa...  11.5 us
    all_to_all x1, blocking collectives, on_device(): lax.all_to_all(dispatch, 'ep', split_axis=0, concat_axis=2, tiled=True)  9.17 us
    all_to_all x1, starting transfers between devices, on_device(): lax.all_to_all(normed, 'ep', split_axis=1, concat_axis=0, tiled=True)  5.19 us
    dot_general x1, matrix products, on_device(): jnp.einsum('shl,slhe->she', weights[..., :positions_all], values, preferr...  4.72 us
    all_to_all x1, waiting for transfers between devices, on_device(): lax.all_to_all(summed.reshape(experts_local, ep_count, capacity, cols), '...  4.66 us
  transfers between devices with their start and end apart: 5, of which 5 were waited for; matrix products, arithmetic and copies ran while one was open for 9% of the time, Pallas kernels for 0%

commit v1 on v0

--- a/solution.py
+++ b/solution.py
@@ -81,8 +81,11 @@
         .reshape(seqs, heads_local * 2 * head_dim)
     )
     term = jnp.dot(head_out, w_output, preferred_element_type=jnp.float32).astype(jnp.bfloat16)
-    attn_sum = lax.psum(
-        lax.optimization_barrier(term).astype(jnp.float32).astype(jnp.bfloat16), "tp"
+    attn_sum = jnp.sum(
+        lax.all_gather(
+            lax.optimization_barrier(term).astype(jnp.float32).astype(jnp.bfloat16), "tp"
+        ),
+        axis=0,
     ).astype(jnp.float32)
     resid = resid_in + attn_sum
     moe_in = rms_scale(resid, moe_gain).astype(jnp.bfloat16)

time: 178 us -> 146 us (0.82)
  waiting for transfers between devices: 102 us -> 70.9 us
    psum x1 -> x0, waiting for transfers between devices: 55 us -> none  [on_device(): lax.psum(lax.optimization_barrier(term).astype(jnp.float32).astype(jnp.bf...]
    all_gather x0 -> x1, waiting for transfers between devices: none -> 21.4 us  [on_device(): lax.all_gather(lax.optimization_barrier(term).astype(jnp.float32).astype(...]
    all_to_all x1, waiting for transfers between devices: 2.22 us -> 4.29 us  [on_device(): lax.all_to_all(normed, 'ep', split_axis=1, concat_axis=0, tiled=True)]
    unnamed x24 -> x28, local copies, waits for them, and re-layouts: 13.1 us -> 12.5 us
  transfers between devices with their start and end apart: 5 -> 5, of which waited for: 5 -> 5; matrix products, arithmetic and copies ran while one was open for 9% -> 10% of each run, Pallas kernels for 0% -> 0%
where the time goes in v1:
time: 146 us; the launch traced here: 145 us
  waiting for transfers between devices  70.9 us (49%)
  matrix products  18.7 us (13%)
  local copies, waits for them, and re-layouts  14.9 us (10%)
  between operations  14 us (10%)
  blocking collectives  9.56 us (7%)
  starting transfers between devices  9 us (6%)
  other arithmetic  8.32 us (6%)
    reduce_scatter x1, waiting for transfers between devices, on_device(): lax.psum_scatter(down.astype(jnp.bfloat16), 'tp', scatter_dimension=2, ti...  28.9 us
    all_gather x1, waiting for transfers between devices, on_device(): lax.all_gather(lax.optimization_barrier(term).astype(jnp.float32).astype(...  21.4 us
    unnamed x28, local copies, waits for them, and re-layouts  12.5 us
    reduce_scatter x1, waiting for transfers between devices, on_device(): lax.psum_scatter(jnp.dot(sliced, stacked, preferred_element_type=jnp.floa...  11.6 us
    all_to_all x1, blocking collectives, on_device(): lax.all_to_all(dispatch, 'ep', split_axis=0, concat_axis=2, tiled=True)  9.56 us
    all_to_all x1, starting transfers between devices, on_device(): lax.all_to_all(normed, 'ep', split_axis=1, concat_axis=0, tiled=True)  5.19 us
    dot_general x1, matrix products, on_device(): jnp.einsum('shl,slhe->she', weights[..., :positions_all], values, preferr...  4.72 us
    all_to_all x1, waiting for transfers between devices, on_device(): lax.all_to_all(summed.reshape(experts_local, ep_count, capacity, cols), '...  4.66 us
  transfers between devices with their start and end apart: 5, of which 5 were waited for; matrix products, arithmetic and copies ran while one was open for 10% of the time, Pallas kernels for 0%

profile of v1, /device:TPU:0, one launch (start us, length us, event | category | flops | bytes accessed | tf_op | source)
XLA Modules:
  0.0 145.4 jit_solution(9317695214894287143)
XLA Ops:
  7.2 1.2 fusion.27
  8.4 1.0 fusion.29
  9.4 0.6 copy.114
  10.0 5.2 %all-to-all-start = ((bf16[16,4,1024]{2,0,1:T(8,128)(2,1)}), bf16[16,4,1024]{2,0,1:T(8,128)(2,1)S(1)}, u32[]{:S(2)}, u32[]{:S(2)}) async-start(bf16[16,4,1024]{2,0,1:T(8,128)(2,1)} %bitcast.81), calls=%async_computation | async-start | bytes 262144 | tf_op jit(solution)/shard_map/all_to_all | solution.py:42
  15.2 0.7 subtract_convert_fusion
  16.0 4.3 %all-to-all-done = bf16[16,4,1024]{2,0,1:T(8,128)(2,1)S(1)} async-done(((bf16[16,4,1024]{2,0,1:T(8,128)(2,1)}), bf16[16,4,1024]{2,0,1:T(8,128)(2,1)S(1)}, u32[]{:S(2)}, u32[]{:S(2)}) %all-to-all-start) | async-done | bytes 131104 | tf_op jit(solution)/shard_map/all_to_all | solution.py:42
  20.3 2.5 %fusion.12 = f32[64,768]{1,0:T(8,128)} fusion(bf16[64,1024]{1,0:T(8,128)(2,1)S(1)} %bitcast.86, bf16[1024,256]{1,0:T(8,128)(2,1)} %param.23, bf16[1024,256]{1,0:T(8,128)(2,1)} %param.22, bf16[1024,256]{1,0:T(8,128)(2,1)} %param.21), kind=kOutput, calls=%fused_computation.16 | convolution fusion | flops 105381888 | bytes 1900544 | tf_op jit(solution)/shard_map/dot_general | solution.py:44
  22.8 0.1 iota_compare_fusion
  22.9 12.3 %copy.78 = bf16[16,1024,256]{1,2,0:T(8,128)(2,1)} copy(bf16[16,1024,256]{2,1,0:T(8,128)(2,1)} %param.27) | data formatting | bytes 16777216 | tf_op args[8]
  35.2 0.1 broadcast_multiply_fusion
  35.3 11.6 %reduce-scatter.3.cloned.1.call-done = f32[16,768]{1,0:T(8,128)} async-done(((f32[64,768]{1,0:T(8,128)}), f32[16,768]{1,0:T(8,128)}) %reduce-scatter.3.cloned.1.call-update) | async-done | bytes 49168 | tf_op jit(solution)/shard_map/reduce_scatter | solution.py:43
  46.9 0.8 convert_element_type.89
  47.7 0.1 reshape.176
  47.8 0.1 reshape.202
  47.9 0.1 reshape.187
  48.0 0.1 multiply_reduce_fusion.2
  48.1 0.1 copy.79
  48.2 4.6 %fusion.3 = f32[2,16,2,1,1024]{4,3,2,1,0:T(1,128)S(1)} fusion(bf16[16,1024,2,2,64]{1,4,3,2,0:T(8,128)(2,1)} %bitcast.82, bf16[16,2,2,64,1]{3,2,1,0,4:T(2,128)(2,1)S(1)} %reshape.202), kind=kOutput, calls=%fused_computation.4 | convolution fusion | flops 8388608 | bytes 8658944 | tf_op jit(solution)/shard_map/shcd,slhcd->cshl/dot_general | solution.py:63
  52.8 0.2 fusion.66
  53.0 0.1 copy.80
  53.1 0.8 fusion.35
  53.9 0.1 fusion.39
  54.0 0.2 copy.93
  54.3 4.7 %fusion = f32[16,2,1,128]{3,2,1,0:T(1,128)S(1)} fusion(bf16[16,2,1024,1]{2,0,1,3:T(8,128)(2,1)S(1)} %slice_bitcast_fusion.2, bf16[16,1024,256]{2,1,0:T(8,128)(2,1)} %param.28), kind=kOutput, calls=%fused_computation.1 | convolution fusion | flops 8388608 | bytes 8470528 | tf_op jit(solution)/shard_map/shl,slhe->she/dot_general | solution.py:72
  59.0 0.2 multiply_reduce_fusion.3
  59.2 0.1 multiply_convert_fusion.2
  59.3 1.0 convolution_convert_fusion.2
  60.5 0.1 copy.82
  60.6 0.1 eq.28
  60.8 0.2 select_reduce_fusion
  61.0 0.1 sub.53
  61.1 0.1 compare_select_fusion
  61.2 0.1 copy.83
  61.4 21.4 %all-gather.3.cloned.1.call-done = bf16[128,4096]{1,0:T(8,128)(2,1)} async-done(((bf16[16,4096]{1,0:T(8,128)(2,1)}), bf16[128,4096]{1,0:T(8,128)(2,1)}) %all-gather.3.cloned.1.call-update) | async-done | bytes 1048592 | tf_op jit(solution)/shard_map/all_gather | solution.py:85
  82.8 1.4 reduce_sum.97
  84.2 0.2 convert_add_fusion
  84.4 0.3 fusion.5
  84.6 9.6 %all_to_all.37 = bf16[4,1,8,4096]{3,2,1,0:T(8,128)(2,1)S(1)} all-to-all(bf16[4,1,8,4096]{3,2,1,0:T(8,128)(2,1)S(1)} %fusion.5), channel_id=1, replica_groups=mesh['ep'=4,'tp'=8] {'ep'}, dimensions={0} | all-to-all | bytes 524288 | tf_op jit(solution)/shard_map/all_to_all | solution.py:109
  94.2 2.0 %fusion.10 = f32[32,256]{1,0:T(8,128)S(1)} fusion(bf16[1,4096,256]{2,1,0:T(8,128)(2,1)} %param.35, bf16[4,1,8,4096]{3,2,1,0:T(8,128)(2,1)S(1)} %all_to_all.37), kind=kOutput, calls=%fused_computation.14 | convolution fusion | flops 67108864 | bytes 2392064 | tf_op jit(solution)/shard_map/erd,edf->erf/dot_general | solution.py:111
  96.3 3.6 %fusion.6 = bf16[1,32,4096]{2,1,0:T(8,128)(2,1)} fusion(bf16[1,256,4096]{2,1,0:T(8,128)(2,1)S(1)} %copy-done, bf16[1,4096,256]{2,1,0:T(8,128)(2,1)} %param.36, bf16[4,1,8,4096]{3,2,1,0:T(8,128)(2,1)S(1)} %all_to_all.37, f32[32,256]{1,0:T(8,128)S(1)} %fusion.10), kind=kOutput, calls=%fused_computation.9 | convolution fusion | flops 134397952 | bytes 4751360 | tf_op jit(solution)/shard_map/erf,efd->erd/dot_general | solution.py:114
  99.9 0.1 reshape.192
  100.1 28.9 %reduce-scatter.5.cloned.1.call-done = bf16[1,32,512]{2,1,0:T(8,128)(2,1)} async-done(((bf16[1,32,4096]{2,1,0:T(8,128)(2,1)}), bf16[1,32,512]{2,1,0:T(8,128)(2,1)}) %reduce-scatter.5.cloned.1.call-update) | async-done | bytes 32784 | tf_op jit(solution)/shard_map/reduce_scatter | solution.py:115
  128.9 3.7 %all-to-all-start.2 = ((bf16[1,4,8,512]{3,2,0,1:T(8,128)(2,1)}), bf16[1,4,8,512]{3,2,0,1:T(8,128)(2,1)S(1)}, u32[]{:S(2)}, u32[]{:S(2)}) async-start(bf16[1,4,8,512]{3,2,0,1:T(8,128)(2,1)} %bitcast.92), calls=%async_computation.4 | async-start | bytes 65536 | tf_op jit(solution)/shard_map/all_to_all | solution.py:117
  132.7 0.1 copy.86
  132.7 4.7 %all-to-all-done.2 = bf16[1,4,8,512]{3,2,0,1:T(8,128)(2,1)S(1)} async-done(((bf16[1,4,8,512]{3,2,0,1:T(8,128)(2,1)}), bf16[1,4,8,512]{3,2,0,1:T(8,128)(2,1)S(1)}, u32[]{:S(2)}, u32[]{:S(2)}) %all-to-all-start.2) | async-done | bytes 32800 | tf_op jit(solution)/shard_map/all_to_all | solution.py:117
  137.4 0.6 gather_fusion
  138.1 0.1 multiply_reduce_fusion.1
  138.2 0.6 add_convert_fusion
  (53 shorter events, 0.7 us)
Async XLA Ops:
  7.2 89.1 %copy-start = (bf16[1,256,4096]{2,1,0:T(8,128)(2,1)S(1)}, bf16[1,256,4096]{2,1,0:T(8,128)(2,1)}, u32[]{:S(2)}) copy-start(bf16[1,256,4096]{2,1,0:T(8,128)(2,1)} %param.37) | copy-start | bytes 6291460
  10.0 10.2 %all-to-all-start = ((bf16[16,4,1024]{2,0,1:T(8,128)(2,1)}), bf16[16,4,1024]{2,0,1:T(8,128)(2,1)S(1)}, u32[]{:S(2)}, u32[]{:S(2)}) async-start(bf16[16,4,1024]{2,0,1:T(8,128)(2,1)} %bitcast.81), calls=%async_computation | async-start | bytes 262144 | tf_op jit(solution)/shard_map/all_to_all | solution.py:42
  15.2 31.6 %reduce-scatter.3.cloned.1.call-start = ((), (), s32[]{:S(2)}) async-start(), calls=%async_computation.5 | async-start | bytes 245760 | tf_op jit(solution)/shard_map/reduce_scatter | solution.py:43
  20.3 2.6 %copy-start.7 = (s32[16]{0:T(128)S(1)}, s32[16]{0:T(128)}, u32[]{:S(2)}) copy-start(s32[16]{0:T(128)} %param.29) | copy-start | bytes 196
  22.8 60.0 %all-gather.3.cloned.1.call-start = ((), (), s32[]{:S(2)}) async-start(), calls=%async_computation.7 | async-start | bytes 1179648 | tf_op jit(solution)/shard_map/all_gather | solution.py:85
  47.7 5.1 %copy-start.4 = (bf16[16,256]{1,0:T(8,128)(2,1)}, bf16[16,256]{1,0:T(8,128)(2,1)S(1)}, u32[]{:S(2)}) copy-start(bf16[16,256]{1,0:T(8,128)(2,1)S(1)} %get-tuple-element.10) | copy-start | bytes 24580
  47.7 6.5 %copy-start.3 = (bf16[16,256]{1,0:T(8,128)(2,1)}, bf16[16,256]{1,0:T(8,128)(2,1)S(1)}, u32[]{:S(2)}) copy-start(bf16[16,256]{1,0:T(8,128)(2,1)S(1)} %get-tuple-element.9) | copy-start | bytes 24580
  52.8 1.1 copy-start.9
  54.2 5.0 %copy-start.10 = (f32[128]{0:T(128)S(1)}, f32[128]{0:T(128)}, u32[]{:S(2)}) copy-start(f32[128]{0:T(128)} %param.25) | copy-start | bytes 1540
  54.3 5.1 %copy-start.2 = (bf16[256,4096]{1,0:T(8,128)(2,1)S(1)}, bf16[256,4096]{1,0:T(8,128)(2,1)}, u32[]{:S(2)}) copy-start(bf16[256,4096]{1,0:T(8,128)(2,1)} %param.26) | copy-start | bytes 6291460
  59.0 1.5 %copy-start.8 = (s32[16,2]{0,1:T(2,128)S(1)}, s32[16,2]{0,1:T(2,128)}, u32[]{:S(2)}) copy-start(s32[16,2]{0,1:T(2,128)} %param.32) | copy-start | bytes 388
  59.0 1.6 %copy-start.12 = (s32[16]{0:T(128)S(1)}, s32[16]{0:T(128)}, u32[]{:S(2)}) copy-start(s32[16]{0:T(128)} %param.31) | copy-start | bytes 196
  59.0 25.2 %copy-start.1 = (bf16[16,4096]{1,0:T(8,128)(2,1)S(1)}, bf16[16,4096]{1,0:T(8,128)(2,1)}, u32[]{:S(2)}) copy-start(bf16[16,4096]{1,0:T(8,128)(2,1)} %param.19) | copy-start | bytes 393220
  59.3 25.0 %copy-start.5 = (f32[4096]{0:T(1024)S(1)}, f32[4096]{0:T(1024)}, u32[]{:S(2)}) copy-start(f32[4096]{0:T(1024)} %param.30) | copy-start | bytes 49156
  60.4 68.5 %reduce-scatter.5.cloned.1.call-start = ((), (), s32[]{:S(2)}) async-start(), calls=%async_computation.6 | async-start | bytes 294912 | tf_op jit(solution)/shard_map/reduce_scatter | solution.py:115
  96.3 3.7 %copy-start.6 = (f32[16,2]{0,1:T(2,128)S(1)}, f32[16,2]{0,1:T(2,128)}, u32[]{:S(2)}) copy-start(f32[16,2]{0,1:T(2,128)} %param.34) | copy-start | bytes 388
  96.3 3.8 %copy-start.11 = (f32[16]{0:T(128)S(1)}, f32[16]{0:T(128)}, u32[]{:S(2)}) copy-start(f32[16]{0:T(128)} %param.33) | copy-start | bytes 196
  128.9 8.5 %all-to-all-start.2 = ((bf16[1,4,8,512]{3,2,0,1:T(8,128)(2,1)}), bf16[1,4,8,512]{3,2,0,1:T(8,128)(2,1)S(1)}, u32[]{:S(2)}, u32[]{:S(2)}) async-start(bf16[1,4,8,512]{3,2,0,1:T(8,128)(2,1)} %bitcast.92), calls=%async_computation.4 | async-start | bytes 65536 | tf_op jit(solution)/shard_map/all_to_all | solution.py:117
Sparse Core Ops, SparseCore 0:
  22.9 23.9 reduce-scatter.2
  60.5 22.2 all-gather.2
  100.0 28.8 reduce-scatter.4
